TPU v7x, 32 devices: a whole 2x2x4 slice. The times are simulated.
32 devices in a mesh: dp: 4 (over y, x), kv: 4 (over z), tp: 2 (over core).
Axes of the slice: x: 2, y: 2, z: 4, core: 2. Of those that a mesh axis runs over, the one named last changes fastest.
Arguments:
- tokens: bfloat16 [16, 4096], P('dp', ('kv', 'tp')), may hold values from -24 to 24
- rec_state: float32 [16, 16, 128, 128], P(('dp', 'kv'), 'tp'), may hold values from -2 to 2
- norm_gain: float32 [4096], replicated, may hold values from 0.1 to 1.9
- w_query: bfloat16 [4096, 2048], P('kv', 'tp'), may hold values from -0.09375 to 0.09375
- w_forget: bfloat16 [4096, 2048], P('kv', 'tp'), may hold values from -0.09375 to 0.09375
- w_input: bfloat16 [4096, 2048], P('kv', 'tp'), may hold values from -0.09375 to 0.09375
- w_outgate: bfloat16 [4096, 2048], P('kv', 'tp'), may hold values from -0.09375 to 0.09375
- lower_bound: float32 [2048], P('tp'), may hold values from 0 to 0.9
- head_gain: float32 [2048], P('tp'), may hold values from 0.1 to 1.9
- w_heads_out: bfloat16 [2048, 4096], P(None, ('kv', 'tp')), may hold values from -0.125 to 0.125
- mixer_gain: float32 [4096], replicated, may hold values from 0.1 to 1.9
- w_gate: bfloat16 [4096, 11264], P(None, ('kv', 'tp')), may hold values from -0.09375 to 0.09375
- w_up: bfloat16 [4096, 11264], P(None, ('kv', 'tp')), may hold values from -0.09375 to 0.09375
- w_down: bfloat16 [11264, 4096], P(('kv', 'tp')), may hold values from -0.078125 to 0.078125
Outputs:
- result: bfloat16 [16, 4096], P('dp', ('kv', 'tp'))
- new_state: float32 [16, 16, 128, 128], P(('dp', 'kv'), 'tp')
All inputs are finite; a program needn't handle non-finite values.
Results may differ from a plain program's by a relative error of at most 0.012.
Values may be sent and summed in bfloat16 or wider, within the bound.
A program may use at most 128 MiB of HBM per device.

v0:
```python
import jax
import jax.numpy as jnp
from jax import lax
from jax.sharding import PartitionSpec as P

HEAD_DIM = 128
epsilon = 1e-06


def channel_mixer(whole_rows, mixer_gain, w_gate, w_up, w_down):
    rows_float = whole_rows.astype(jnp.float32)
    mixer_scale = lax.rsqrt(jnp.mean(rows_float * rows_float, axis=1, keepdims=True) + epsilon)
    normed = (rows_float * mixer_scale * mixer_gain).astype(jnp.bfloat16)
    gate_val = jnp.dot(normed, w_gate, preferred_element_type=jnp.float32)
    up_val = jnp.dot(normed, w_up, preferred_element_type=jnp.float32)
    hidden = (jax.nn.silu(gate_val) * up_val).astype(jnp.bfloat16)
    return jnp.dot(hidden, w_down, preferred_element_type=jnp.float32)


def local(
    tokens,
    rec_state,
    norm_gain,
    w_query,
    w_forget,
    w_input,
    w_outgate,
    lower_bound,
    head_gain,
    w_heads_out,
    mixer_gain,
    w_gate,
    w_up,
    w_down,
):
    kv_count = lax.axis_size("kv")
    tp_count = lax.axis_size("tp")
    kv_index = lax.axis_index("kv")
    row_count = tokens.shape[0]
    seq_count = rec_state.shape[0]
    model_width = norm_gain.shape[0]
    col_block = model_width // kv_count
    tok_float = tokens.astype(jnp.float32)
    whole_rows = lax.all_gather(tokens, ("kv", "tp"), axis=1, tiled=True).astype(jnp.float32)
    squares = jnp.sum(whole_rows * whole_rows, axis=1)
    own_cols = lax.dynamic_slice_in_dim(whole_rows, kv_index * col_block, col_block, 1)
    gain_block = lax.dynamic_slice_in_dim(norm_gain, kv_index * col_block, col_block, 0)
    scaled = (own_cols * gain_block).astype(jnp.bfloat16)
    projected = lax.psum_scatter(
        jnp.stack(
            [
                jnp.dot(scaled, weight, preferred_element_type=jnp.float32)
                for weight in (w_query, w_forget, w_input, w_outgate)
            ],
            axis=1,
        ),
        "kv",
        scatter_dimension=0,
        tiled=True,
    )
    my_squares = lax.dynamic_slice_in_dim(squares, kv_index * seq_count, seq_count, 0)
    row_scale = lax.rsqrt(my_squares / model_width + epsilon)[:, None]
    query_pre = row_scale * projected[:, 0]
    forget_pre = row_scale * projected[:, 1]
    value_in = row_scale * projected[:, 2]
    gate_pre = row_scale * projected[:, 3]
    forget = lower_bound + (1.0 - lower_bound) * jax.nn.sigmoid(forget_pre)
    key_in = 1.0 - forget
    query_act = jax.nn.silu(query_pre)
    head_count = rec_state.shape[1]
    shaped = (seq_count, head_count, HEAD_DIM)
    forget = forget.reshape(shaped)
    key_in = key_in.reshape(shaped)
    value_in = value_in.reshape(shaped)
    query_act = query_act.reshape(shaped)
    new_state = forget[:, :, :, None] * rec_state + key_in[:, :, :, None] * value_in[:, :, None, :]
    head_out = jnp.sum(query_act[:, :, :, None] * new_state, axis=2)
    head_out = head_out * lax.rsqrt(jnp.mean(head_out * head_out, axis=2, keepdims=True) + epsilon)
    head_out = head_out * head_gain.reshape(head_count, HEAD_DIM)
    local_width = head_count * HEAD_DIM
    gated = (head_out.reshape(seq_count, local_width) * jax.nn.silu(gate_pre)).astype(jnp.bfloat16)
    every_head = lax.all_gather(gated[None], ("kv", "tp"), axis=0, tiled=True)
    every_head = every_head.reshape(kv_count, tp_count, seq_count, local_width)
    every_head = every_head.transpose(0, 2, 1, 3).reshape(
        kv_count * seq_count, tp_count * local_width
    )
    mixed_add = jnp.dot(every_head, w_heads_out, preferred_element_type=jnp.float32)
    mixed = (tok_float + mixed_add).astype(jnp.bfloat16)
    gathered = lax.all_gather(mixed, ("kv", "tp"), axis=1, tiled=True)
    terms = channel_mixer(gathered, mixer_gain, w_gate, w_up, w_down)
    out_block = model_width // (kv_count * tp_count)
    blocked = terms.reshape(row_count, kv_count, tp_count, out_block)
    chip_sum = lax.psum_scatter(blocked.astype(jnp.bfloat16), "tp", scatter_dimension=2, tiled=True)
    down_sum = (
        lax.psum_scatter(chip_sum, "kv", scatter_dimension=1, tiled=True)
        .astype(jnp.float32)
        .reshape(row_count, out_block)
    )
    result = (mixed.astype(jnp.float32) + down_sum).astype(jnp.bfloat16)
    return (result, new_state)


def solution(mesh):
    placed = (
        P("dp", ("kv", "tp")),
        P(("dp", "kv"), "tp", None, None),
        P(),
        P("kv", "tp"),
        P("kv", "tp"),
        P("kv", "tp"),
        P("kv", "tp"),
        P("tp"),
        P("tp"),
        P(None, ("kv", "tp")),
        P(),
        P(None, ("kv", "tp")),
        P(None, ("kv", "tp")),
        P(("kv", "tp"), None),
    )
    return jax.shard_map(
        local,
        mesh=mesh,
        in_specs=placed,
        out_specs=(P("dp", ("kv", "tp")), P(("dp", "kv"), "tp", None, None)),
        check_vma=False,
    )
```

profile of v0, /device:TPU:0, one launch (start us, length us, event | category | flops | bytes accessed | tf_op | source)
XLA Modules:
  0.0 140.6 jit_solution(1454577620565583170)
XLA Ops:
  7.2 0.0 copy-start
  7.2 0.0 all-reduce.5.cloned.1.call-start
  7.2 16.1 %all_gather.9 = bf16[4,4096]{1,0:T(4,128)(2,1)S(1)} all-gather(bf16[4,512]{1,0:T(4,128)(2,1)} %param.14), channel_id=1, replica_groups=mesh['dp'=4,'kv'=4,'tp'=2] {'kv','tp'}, dimensions={1}, use_global_device_ids=true | all-gather | bytes 36864 | tf_op jit(solution)/shard_map/all_gather | solution.py:44
  23.3 0.0 copy-start.1
  23.3 0.8 dynamic_slice.11
  24.2 0.0 copy-done
  24.2 0.0 copy-start.2
  24.2 0.4 convolution_bitcast_fusion
  24.6 0.3 copy-done.1
  24.9 0.0 copy-start.3
  24.9 0.4 convolution_bitcast_fusion.1
  25.3 0.6 copy-done.2
  25.9 0.0 copy-start.10
  25.9 0.0 copy-start.9
  25.9 0.0 copy-start.7
  25.9 0.0 copy-start.4
  25.9 0.4 convolution_bitcast_fusion.2
  26.3 0.3 copy-done.3
  26.6 0.0 copy-start.8
  26.7 0.0 copy-start.6
  26.7 0.4 convolution_bitcast_fusion.3
  27.0 0.0 copy-start.5
  27.1 0.7 copy.18
  27.7 0.0 all-reduce.5.cloned.1.call-update
  27.8 0.0 copy-done.10
  27.8 0.6 dynamic-slice.2
  28.4 0.0 copy-done.9
  28.4 0.6 dynamic-slice
  29.0 0.1 multiply_reduce_fusion.1
  29.1 0.6 dynamic_slice.9
  30.4 32.8 %all-reduce.5.cloned.1.call-done = f32[4,4,1024]{2,1,0:T(4,128)} async-done(((f32[4,4,1024]{2,1,0:T(4,128)}), f32[4,4,1024]{2,1,0:T(4,128)}) %all-reduce.5.cloned.1.call-update) | async-done | bytes 65552
  63.2 1.5 %dynamic-slice_multiply_fusion = (f32[1,1,1024]{2,1,0:T(1,128)S(1)}, f32[1,1,1024]{2,1,0:T(1,128)S(1)}, f32[1,1,1024]{2,1,0:T(1,128)S(1)}, f32[1,1,1024]{2,1,0:T(1,128)S(1)}) fusion(f32[4,4,1024]{2,1,0:T(4,128)} %all-reduce.5.cloned.1.call-done, u32[]{:T(128)} %bitcast.19, u32[]{:T(128)S(6)} %convert.4, f32[]{:T(128)} %bitcast, u32[]{:T(128)S(6)} %convert.3, ...), kind=kLoop, calls=%fused_computation.26 | loop fusion | flops 7168 | bytes 32788 | tf_op jit(solution)/shard_map/mul | solution.py:66
  64.7 0.0 copy-done.7
  64.7 0.0 copy-done.4
  64.8 1.3 multiply_reduce_fusion
  66.0 0.1 multiply_reduce_fusion.2
  66.1 0.1 mul.206
  66.2 0.0 copy-done.8
  66.2 12.8 %all-gather = bf16[8192]{0:T(1024)(128)(2,1)S(1)} all-gather(bf16[1024]{0:T(1024)(128)(2,1)S(1)} %fusion.13), channel_id=2, replica_groups=mesh['dp'=4,'kv'=4,'tp'=2] {'kv','tp'}, dimensions={0}, use_global_device_ids=true | all-gather | bytes 18432 | tf_op jit(solution)/shard_map/all_gather | solution.py:82
  79.0 0.0 copy-done.6
  79.0 2.0 %fusion.1 = bf16[4,512]{1,0:T(4,128)(2,1)S(1)} fusion(bf16[4,2048]{1,0:T(4,128)(2,1)S(1)} %reshape_transpose_reshape.3, bf16[2048,512]{1,0:T(8,128)(2,1)} %param.23, bf16[4,512]{1,0:T(4,128)(2,1)S(1)} %copy-done.6), kind=kOutput, calls=%fused_computation.8 | convolution fusion | flops 8394752 | bytes 2121728 | tf_op jit(solution)/shard_map/dot_general | solution.py:87
  81.0 14.1 %all_gather.11 = bf16[4,4096]{1,0:T(4,128)(2,1)S(1)} all-gather(bf16[4,512]{1,0:T(4,128)(2,1)S(1)} %fusion.1), channel_id=1, replica_groups=mesh['dp'=4,'kv'=4,'tp'=2] {'kv','tp'}, dimensions={1}, use_global_device_ids=true | all-gather | bytes 36864 | tf_op jit(solution)/shard_map/all_gather | solution.py:89
  95.1 0.1 fusion.2
  95.2 0.0 copy-done.5
  95.2 5.9 %fusion.18 = f32[4,1408]{1,0:T(4,128)S(1)} fusion(bf16[4096,1408]{1,0:T(8,128)(2,1)} %param.25, bf16[4,4096]{1,0:T(4,128)(2,1)S(1)} %all_gather.11, f32[4096]{0:T(1024)S(1)} %copy-done.5, f32[4]{0:T(128)S(1)} %add_rsqrt_fusion), kind=kOutput, calls=%fused_computation.45 | convolution fusion | flops 46202880 | bytes 11606032 | tf_op jit(solution)/shard_map/dot_general | solution.py:14
  101.1 11.0 %convolution_convert_fusion = bf16[4,4096]{1,0:T(4,128)(2,1)S(1)} fusion(bf16[1408,4096]{1,0:T(8,128)(2,1)} %param.27, bf16[4096,1408]{1,0:T(8,128)(2,1)} %param.26, f32[4,1408]{1,0:T(4,128)S(1)} %fusion.18, bf16[4,4096]{1,0:T(4,128)(2,1)S(1)} %all_gather.11, f32[4096]{0:T(1024)S(1)} %copy-done.5, f32[4]{0:T(128)S(1)} %add_rsqrt_fusion), kind=kOutput, calls=%fused_computation | convolution fusion | flops 92390400 | bytes 23173136 | tf_op jit(solution)/shard_map/dot_general | solution.py:17
  112.1 3.6 %all-reduce.1 = bf16[4,4,2,512]{3,0,2,1:T(4,128)(2,1)S(1)} all-reduce(bf16[4,4,2,512]{3,0,2,1:T(4,128)(2,1)S(1)} %bitcast.49), channel_id=4, replica_groups=mesh['dp'=4,'kv'=4,'tp'=2] {'tp'}, use_global_device_ids=true, to_apply=%region_5.6.clone | all-reduce | flops 16384 | bytes 65536
  115.7 0.6 constant_dynamic-slice_fusion
  116.4 16.2 %all-reduce.2 = bf16[4,4,1,512]{3,0,2,1:T(4,128)(2,1)S(1)} all-reduce(bf16[4,4,1,512]{3,0,2,1:T(4,128)(2,1)S(1)} %constant_dynamic-slice_fusion), channel_id=5, replica_groups=mesh['dp'=4,'kv'=4,'tp'=2] {'kv'}, use_global_device_ids=true, to_apply=%region_6.7.clone | all-reduce | flops 8192 | bytes 32768
  132.6 1.2 fusion.9
  (9 shorter events, 0.1 us)
Async XLA Ops:
  7.2 17.0 %copy-start = (bf16[1024,1024]{1,0:T(8,128)(2,1)S(1)}, bf16[1024,1024]{1,0:T(8,128)(2,1)}, u32[]{:S(2)}) copy-start(bf16[1024,1024]{1,0:T(8,128)(2,1)} %param.20) | copy-start | bytes 6291460
  7.2 56.0 %all-reduce.5.cloned.1.call-start = ((), (), s32[]{:S(2)}) async-start(), calls=%async_computation | async-start | bytes 131072
  23.3 1.6 %copy-start.1 = (bf16[1024,1024]{1,0:T(8,128)(2,1)S(1)}, bf16[1024,1024]{1,0:T(8,128)(2,1)}, u32[]{:S(2)}) copy-start(bf16[1024,1024]{1,0:T(8,128)(2,1)} %param.19) | copy-start | bytes 6291460
  24.2 1.8 %copy-start.2 = (bf16[1024,1024]{1,0:T(8,128)(2,1)S(1)}, bf16[1024,1024]{1,0:T(8,128)(2,1)}, u32[]{:S(2)}) copy-start(bf16[1024,1024]{1,0:T(8,128)(2,1)} %param.18) | copy-start | bytes 6291460
  24.9 1.7 %copy-start.3 = (bf16[1024,1024]{1,0:T(8,128)(2,1)S(1)}, bf16[1024,1024]{1,0:T(8,128)(2,1)}, u32[]{:S(2)}) copy-start(bf16[1024,1024]{1,0:T(8,128)(2,1)} %param.17) | copy-start | bytes 6291460
  25.9 1.8 %copy-start.10 = (u32[32]{0:T(128)S(1)}, u32[32]{0:T(128)}, u32[]{:S(2)}) copy-start(u32[32]{0:T(128)} %constant.45) | copy-start | bytes 388
  25.9 2.4 %copy-start.9 = (u32[32]{0:T(128)S(1)}, u32[32]{0:T(128)}, u32[]{:S(2)}) copy-start(u32[32]{0:T(128)} %constant.41) | copy-start | bytes 388
  25.9 38.8 %copy-start.7 = (f32[1024]{0:T(1024)S(1)}, f32[1024]{0:T(1024)}, u32[]{:S(2)}) copy-start(f32[1024]{0:T(1024)} %param.21) | copy-start | bytes 12292
  25.9 38.8 %copy-start.4 = (f32[1,8,128,128]{3,2,1,0:T(8,128)S(1)}, f32[1,8,128,128]{3,2,1,0:T(8,128)}, u32[]{:S(2)}) copy-start(f32[1,8,128,128]{3,2,1,0:T(8,128)} %param.15) | copy-start | bytes 1572868
  26.6 39.6 %copy-start.8 = (f32[1024]{0:T(1024)S(1)}, f32[1024]{0:T(1024)}, u32[]{:S(2)}) copy-start(f32[1024]{0:T(1024)} %param.22) | copy-start | bytes 12292
  26.7 52.4 %copy-start.6 = (bf16[4,512]{1,0:T(4,128)(2,1)S(1)}, bf16[4,512]{1,0:T(4,128)(2,1)}, u32[]{:S(2)}) copy-start(bf16[4,512]{1,0:T(4,128)(2,1)} %param.14) | copy-start | bytes 12292
  27.0 68.2 %copy-start.5 = (f32[4096]{0:T(1024)S(1)}, f32[4096]{0:T(1024)}, u32[]{:S(2)}) copy-start(f32[4096]{0:T(1024)} %param.24) | copy-start | bytes 49156
Sparse Core Ops, SparseCore 0:
  27.9 35.2 all-reduce.4
where the time goes:
time: 141 us
  blocking collectives  62.7 us (44%)
  waiting for transfers between devices  32.8 us (23%)
  matrix products  20.4 us (14%)
  between operations  14.9 us (11%)
  local copies, waits for them, and re-layouts  5.37 us (4%)
  other arithmetic  4.46 us (3%)
    unnamed x2, waiting for transfers between devices  32.8 us
    unnamed x2, blocking collectives  19.8 us
    all_gather x1, blocking collectives, local(): lax.all_gather(tokens, ('kv', 'tp'), axis=1, tiled=True).astype(jnp.float32)  16.1 us
    all_gather x1, blocking collectives, local(): gathered = lax.all_gather(mixed, ('kv', 'tp'), axis=1, tiled=True)  14.1 us
    all_gather x1, blocking collectives, local(): every_head = lax.all_gather(gated[None], ('kv', 'tp'), axis=0, tiled=True)  12.8 us
    dot_general x1, matrix products, channel_mixer(): return jnp.dot(hidden, w_down, preferred_element_type=jnp.float32)  11 us
    dot_general x1, matrix products, channel_mixer(): gate_val = jnp.dot(normed, w_gate, preferred_element_type=jnp.float32)  5.9 us
    unnamed x25, local copies, waits for them, and re-layouts  3.18 us
  transfers between devices with their start and end apart: 1, of which 1 were waited for; matrix products, arithmetic and copies ran while one was open for 1% of the time, Pallas kernels for 0%

commit v1 on v0

--- a/solution.py
+++ b/solution.py
@@ -5,6 +5,13 @@
 
 HEAD_DIM = 128
 epsilon = 1e-06
+
+
+def swapped_in(x, axis, d):
+    devices = lax.axis_size(axis)
+    blocks = jnp.stack([x for _ in range(devices)])
+    blocks = lax.all_to_all(blocks, axis, split_axis=0, concat_axis=0)
+    return jnp.concatenate(blocks, axis=d)
 
 
 def channel_mixer(whole_rows, mixer_gain, w_gate, w_up, w_down):
@@ -41,7 +48,7 @@
     model_width = norm_gain.shape[0]
     col_block = model_width // kv_count
     tok_float = tokens.astype(jnp.float32)
-    whole_rows = lax.all_gather(tokens, ("kv", "tp"), axis=1, tiled=True).astype(jnp.float32)
+    whole_rows = swapped_in(tokens, ("kv", "tp"), 1).astype(jnp.float32)
     squares = jnp.sum(whole_rows * whole_rows, axis=1)
     own_cols = lax.dynamic_slice_in_dim(whole_rows, kv_index * col_block, col_block, 1)
     gain_block = lax.dynamic_slice_in_dim(norm_gain, kv_index * col_block, col_block, 0)

time: 141 us -> 136 us (0.965)
  blocking collectives: 62.7 us -> 46.6 us
  starting transfers between devices: 0.04 us -> 6.39 us
  local copies, waits for them, and re-layouts: 5.37 us -> 8.81 us
  waiting for transfers between devices: 32.8 us -> 34.5 us
    all_gather x1 -> x0, blocking collectives: 16.1 us -> none  [local(): lax.all_gather(tokens, ('kv', 'tp'), axis=1, tiled=True).astype(jnp.float32)]
    all_to_all x0 -> x1, starting transfers between devices: none -> 6.35 us  [swapped_in(): blocks = lax.all_to_all(blocks, axis, split_axis=0, concat_axis=0)]
    all_to_all x0 -> x1, waiting for transfers between devices: none -> 2.48 us  [swapped_in(): blocks = lax.all_to_all(blocks, axis, split_axis=0, concat_axis=0)]
    unnamed x25 -> x21, local copies, waits for them, and re-layouts: 3.18 us -> 5.31 us
    another operation x0 -> x1, local copies, waits for them, and re-layouts: none -> 1.46 us  [swapped_in(): blocks = jnp.stack([x for _ in range(devices)])]
  transfers between devices with their start and end apart: 1 -> 2, of which waited for: 1 -> 2; matrix products, arithmetic and copies ran while one was open for 1% -> 3% of each run, Pallas kernels for 0% -> 0%
where the time goes in v1:
time: 136 us
  blocking collectives  46.6 us (34%)
  waiting for transfers between devices  34.5 us (25%)
  matrix products  20.4 us (15%)
  between operations  14.8 us (11%)
  local copies, waits for them, and re-layouts  8.81 us (6%)
  starting transfers between devices  6.39 us (5%)
  other arithmetic  4.46 us (3%)
    unnamed x2, waiting for transfers between devices  32 us
    unnamed x2, blocking collectives  19.8 us
    all_gather x1, blocking collectives, local(): gathered = lax.all_gather(mixed, ('kv', 'tp'), axis=1, tiled=True)  14.1 us
    all_gather x1, blocking collectives, local(): every_head = lax.all_gather(gated[None], ('kv', 'tp'), axis=0, tiled=True)  12.8 us
    dot_general x1, matrix products, channel_mixer(): return jnp.dot(hidden, w_down, preferred_element_type=jnp.float32)  11 us
    all_to_all x1, starting transfers between devices, swapped_in(): blocks = lax.all_to_all(blocks, axis, split_axis=0, concat_axis=0)  6.35 us
    dot_general x1, matrix products, channel_mixer(): gate_val = jnp.dot(normed, w_gate, preferred_element_type=jnp.float32)  5.9 us
    unnamed x21, local copies, waits for them, and re-layouts  5.31 us
  transfers between devices with their start and end apart: 2, of which 2 were waited for; matrix products, arithmetic and copies ran while one was open for 3% of the time, Pallas kernels for 0%

profile of v1, /device:TPU:0, one launch (start us, length us, event | category | flops | bytes accessed | tf_op | source)
XLA Modules:
  0.0 136.0 jit_solution(8624220324888958929)
XLA Ops:
  7.2 0.0 copy-start
  7.2 1.5 %stack.12 = bf16[8,4,512]{2,1,0:T(4,128)(2,1)} broadcast(bf16[4,512]{1,0:T(4,128)(2,1)} %param.14), dimensions={1,2} | broadcast | bytes 36864 | tf_op jit(solution)/shard_map/stack | solution.py:12
  8.6 6.4 %all-to-all-start = ((bf16[8,4,512]{2,1,0:T(4,128)(2,1)}), bf16[8,4,512]{2,1,0:T(4,128)(2,1)S(1)}, u32[]{:S(2)}, u32[]{:S(2)}) async-start(bf16[8,4,512]{2,1,0:T(4,128)(2,1)} %stack.12), calls=%async_computation | async-start | bytes 65536 | tf_op jit(solution)/shard_map/all_to_all | solution.py:13
  15.0 0.0 all-reduce.5.cloned.1.call-start
  15.0 1.3 dynamic-slice.2
  16.3 1.3 dynamic-slice
  17.6 0.7 dynamic_slice.11
  18.3 2.5 %all-to-all-done = bf16[8,4,512]{2,1,0:T(4,128)(2,1)S(1)} async-done(((bf16[8,4,512]{2,1,0:T(4,128)(2,1)}), bf16[8,4,512]{2,1,0:T(4,128)(2,1)S(1)}, u32[]{:S(2)}, u32[]{:S(2)}) %all-to-all-start) | async-done | bytes 32800 | tf_op jit(solution)/shard_map/all_to_all | solution.py:13
  20.7 0.0 copy-start.1
  20.8 0.0 copy-done
  20.8 0.0 copy-start.2
  20.8 0.4 convolution_bitcast_fusion
  21.2 1.2 copy-done.1
  22.3 0.0 copy-start.3
  22.3 0.4 convolution_bitcast_fusion.1
  22.7 0.3 copy-done.2
  23.0 0.0 copy-start.7
  23.0 0.0 copy-start.4
  23.0 0.4 convolution_bitcast_fusion.2
  23.4 0.7 copy-done.3
  24.1 0.0 copy-start.8
  24.1 0.0 copy-start.6
  24.1 0.4 convolution_bitcast_fusion.3
  24.5 0.0 copy-start.5
  24.5 0.7 copy.21
  25.2 0.0 all-reduce.5.cloned.1.call-update
  25.2 0.1 multiply_reduce_fusion.1
  25.3 0.6 dynamic_slice.9
  26.6 32.0 %all-reduce.5.cloned.1.call-done = f32[4,4,1024]{2,1,0:T(4,128)} async-done(((f32[4,4,1024]{2,1,0:T(4,128)}), f32[4,4,1024]{2,1,0:T(4,128)}) %all-reduce.5.cloned.1.call-update) | async-done | bytes 65552
  58.6 1.5 %dynamic-slice_multiply_fusion = (f32[1,1,1024]{2,1,0:T(1,128)S(1)}, f32[1,1,1024]{2,1,0:T(1,128)S(1)}, f32[1,1,1024]{2,1,0:T(1,128)S(1)}, f32[1,1,1024]{2,1,0:T(1,128)S(1)}) fusion(f32[4,4,1024]{2,1,0:T(4,128)} %all-reduce.5.cloned.1.call-done, u32[]{:T(128)} %bitcast.22, u32[]{:T(128)S(6)} %convert.6, f32[]{:T(128)} %bitcast, u32[]{:T(128)S(6)} %convert.5, ...), kind=kLoop, calls=%fused_computation.26 | loop fusion | flops 7168 | bytes 32788 | tf_op jit(solution)/shard_map/mul | solution.py:73
  60.1 0.0 copy-done.7
  60.1 0.0 copy-done.4
  60.1 1.3 multiply_reduce_fusion
  61.4 0.1 multiply_reduce_fusion.2
  61.5 0.1 mul.208
  61.6 0.0 copy-done.8
  61.6 12.8 %all-gather = bf16[8192]{0:T(1024)(128)(2,1)S(1)} all-gather(bf16[1024]{0:T(1024)(128)(2,1)S(1)} %fusion.13), channel_id=2, replica_groups=mesh['dp'=4,'kv'=4,'tp'=2] {'kv','tp'}, dimensions={0}, use_global_device_ids=true | all-gather | bytes 18432 | tf_op jit(solution)/shard_map/all_gather | solution.py:89
  74.4 0.0 copy-done.6
  74.4 2.0 %fusion.1 = bf16[4,512]{1,0:T(4,128)(2,1)S(1)} fusion(bf16[4,2048]{1,0:T(4,128)(2,1)S(1)} %reshape_transpose_reshape.3, bf16[2048,512]{1,0:T(8,128)(2,1)} %param.23, bf16[4,512]{1,0:T(4,128)(2,1)S(1)} %copy-done.6), kind=kOutput, calls=%fused_computation.8 | convolution fusion | flops 8394752 | bytes 2121728 | tf_op jit(solution)/shard_map/dot_general | solution.py:94
  76.4 14.1 %all_gather.7 = bf16[4,4096]{1,0:T(4,128)(2,1)S(1)} all-gather(bf16[4,512]{1,0:T(4,128)(2,1)S(1)} %fusion.1), channel_id=1, replica_groups=mesh['dp'=4,'kv'=4,'tp'=2] {'kv','tp'}, dimensions={1}, use_global_device_ids=true | all-gather | bytes 36864 | tf_op jit(solution)/shard_map/all_gather | solution.py:96
  90.5 0.1 fusion.2
  90.6 0.0 copy-done.5
  90.6 5.9 %fusion.18 = f32[4,1408]{1,0:T(4,128)S(1)} fusion(bf16[4096,1408]{1,0:T(8,128)(2,1)} %param.25, bf16[4,4096]{1,0:T(4,128)(2,1)S(1)} %all_gather.7, f32[4096]{0:T(1024)S(1)} %copy-done.5, f32[4]{0:T(128)S(1)} %add_rsqrt_fusion), kind=kOutput, calls=%fused_computation.45 | convolution fusion | flops 46202880 | bytes 11606032 | tf_op jit(solution)/shard_map/dot_general | solution.py:21
  96.5 11.0 %convolution_convert_fusion = bf16[4,4096]{1,0:T(4,128)(2,1)S(1)} fusion(bf16[1408,4096]{1,0:T(8,128)(2,1)} %param.27, bf16[4096,1408]{1,0:T(8,128)(2,1)} %param.26, f32[4,1408]{1,0:T(4,128)S(1)} %fusion.18, bf16[4,4096]{1,0:T(4,128)(2,1)S(1)} %all_gather.7, f32[4096]{0:T(1024)S(1)} %copy-done.5, f32[4]{0:T(128)S(1)} %add_rsqrt_fusion), kind=kOutput, calls=%fused_computation | convolution fusion | flops 92390400 | bytes 23173136 | tf_op jit(solution)/shard_map/dot_general | solution.py:24
  107.5 3.6 %all-reduce.1 = bf16[4,4,2,512]{3,0,2,1:T(4,128)(2,1)S(1)} all-reduce(bf16[4,4,2,512]{3,0,2,1:T(4,128)(2,1)S(1)} %bitcast.52), channel_id=4, replica_groups=mesh['dp'=4,'kv'=4,'tp'=2] {'tp'}, use_global_device_ids=true, to_apply=%region_5.6.clone | all-reduce | flops 16384 | bytes 65536
  111.1 0.6 constant_dynamic-slice_fusion
  111.8 16.2 %all-reduce.2 = bf16[4,4,1,512]{3,0,2,1:T(4,128)(2,1)S(1)} all-reduce(bf16[4,4,1,512]{3,0,2,1:T(4,128)(2,1)S(1)} %constant_dynamic-slice_fusion), channel_id=5, replica_groups=mesh['dp'=4,'kv'=4,'tp'=2] {'kv'}, use_global_device_ids=true, to_apply=%region_6.7.clone | all-reduce | flops 8192 | bytes 32768
  127.9 1.2 fusion.9
  (9 shorter events, 0.1 us)
Async XLA Ops:
  7.2 13.6 %copy-start = (bf16[1024,1024]{1,0:T(8,128)(2,1)S(1)}, bf16[1024,1024]{1,0:T(8,128)(2,1)}, u32[]{:S(2)}) copy-start(bf16[1024,1024]{1,0:T(8,128)(2,1)} %param.20) | copy-start | bytes 6291460
  8.6 12.1 %all-to-all-start = ((bf16[8,4,512]{2,1,0:T(4,128)(2,1)}), bf16[8,4,512]{2,1,0:T(4,128)(2,1)S(1)}, u32[]{:S(2)}, u32[]{:S(2)}) async-start(bf16[8,4,512]{2,1,0:T(4,128)(2,1)} %stack.12), calls=%async_computation | async-start | bytes 65536 | tf_op jit(solution)/shard_map/all_to_all | solution.py:13
  15.0 43.6 %all-reduce.5.cloned.1.call-start = ((), (), s32[]{:S(2)}) async-start(), calls=%async_computation.1 | async-start | bytes 131072
  20.7 1.6 %copy-start.1 = (bf16[1024,1024]{1,0:T(8,128)(2,1)S(1)}, bf16[1024,1024]{1,0:T(8,128)(2,1)}, u32[]{:S(2)}) copy-start(bf16[1024,1024]{1,0:T(8,128)(2,1)} %param.19) | copy-start | bytes 6291460
  20.8 2.2 %copy-start.2 = (bf16[1024,1024]{1,0:T(8,128)(2,1)S(1)}, bf16[1024,1024]{1,0:T(8,128)(2,1)}, u32[]{:S(2)}) copy-start(bf16[1024,1024]{1,0:T(8,128)(2,1)} %param.18) | copy-start | bytes 6291460
  22.3 1.7 %copy-start.3 = (bf16[1024,1024]{1,0:T(8,128)(2,1)S(1)}, bf16[1024,1024]{1,0:T(8,128)(2,1)}, u32[]{:S(2)}) copy-start(bf16[1024,1024]{1,0:T(8,128)(2,1)} %param.17) | copy-start | bytes 6291460
  23.0 37.1 %copy-start.7 = (f32[1024]{0:T(1024)S(1)}, f32[1024]{0:T(1024)}, u32[]{:S(2)}) copy-start(f32[1024]{0:T(1024)} %param.21) | copy-start | bytes 12292
  23.0 37.2 %copy-start.4 = (f32[1,8,128,128]{3,2,1,0:T(8,128)S(1)}, f32[1,8,128,128]{3,2,1,0:T(8,128)}, u32[]{:S(2)}) copy-start(f32[1,8,128,128]{3,2,1,0:T(8,128)} %param.15) | copy-start | bytes 1572868
  24.1 37.5 %copy-start.8 = (f32[1024]{0:T(1024)S(1)}, f32[1024]{0:T(1024)}, u32[]{:S(2)}) copy-start(f32[1024]{0:T(1024)} %param.22) | copy-start | bytes 12292
  24.1 50.3 %copy-start.6 = (bf16[4,512]{1,0:T(4,128)(2,1)S(1)}, bf16[4,512]{1,0:T(4,128)(2,1)}, u32[]{:S(2)}) copy-start(bf16[4,512]{1,0:T(4,128)(2,1)} %param.14) | copy-start | bytes 12292
  24.5 66.2 %copy-start.5 = (f32[4096]{0:T(1024)S(1)}, f32[4096]{0:T(1024)}, u32[]{:S(2)}) copy-start(f32[4096]{0:T(1024)} %param.24) | copy-start | bytes 49156
Sparse Core Ops, SparseCore 0:
  25.3 33.2 all-reduce.4
